TPU v7x, 32 devices: a whole 2x2x4 slice. The times are simulated.
32 devices in a mesh: ep: 8 (over z, y), tp: 4 (over x, core).
Axes of the slice: x: 2, y: 2, z: 4, core: 2. Of those that a mesh axis runs over, the one named last changes fastest.
Arguments:
- mixer_input: bfloat16 [4096, 2048], P(('ep', 'tp')), may hold values from -6 to 6
- expert_input: bfloat16 [4096, 2048], P(('ep', 'tp')), may hold values from -6 to 6
- mixer_gain: float32 [2048], replicated, may hold values from 0.1 to 1.9
- query_down: bfloat16 [2048, 1536], replicated, may hold values from -0.125 to 0.125
- latent_down: bfloat16 [2048, 512], replicated, may hold values from -0.125 to 0.125
- rotary_down: bfloat16 [2048, 32], replicated, may hold values from -0.125 to 0.125
- query_gain: float32 [1536], replicated, may hold values from 0.8 to 40, as said below
- latent_gain: float32 [512], replicated, may hold values from 0.1 to 1.9
- query_plain: bfloat16 [1536, 1024], P(None, 'tp'), may hold values from -0.15625 to 0.15625
- query_rotary: bfloat16 [1536, 512], P(None, 'tp'), may hold values from -0.15625 to 0.15625
- key_plain: bfloat16 [512, 1024], P(None, 'tp'), may hold values from -0.25 to 0.25
- value_up: bfloat16 [512, 1024], P(None, 'tp'), may hold values from -0.25 to 0.25
- output_proj: bfloat16 [1024, 2048], P('tp'), may hold values from -0.1875 to 0.1875
- mixed_gain: float32 [2048], replicated, may hold values from 0.1 to 1.9
- expert_norm: float32 [2048], replicated, may hold values from 0.1 to 1.9
- route_ids: int32 [4096, 2], P(('ep', 'tp')), may hold values from 0 to 7, all different within a row; in each aligned block of 128 rows (0 to 127, 128 to 255, ...) at most 40 rows name the same one
- route_weight: float32 [4096, 2], P(('ep', 'tp')), may hold values from 0.2 to 1
- gate_proj: bfloat16 [8, 2048, 2048], P('ep', None, 'tp'), may hold values from -0.3984375 to 0.3984375
- up_proj: bfloat16 [8, 2048, 2048], P('ep', None, 'tp'), may hold values from -0.3984375 to 0.3984375
- down_proj: bfloat16 [8, 2048, 2048], P('ep', 'tp'), may hold values from -0.125 to 0.125
- expert_gain: float32 [2048], replicated, may hold values from 0.1 to 1.9
Outputs:
- mixer_out: bfloat16 [4096, 2048], P(('ep', 'tp'))
- expert_out: bfloat16 [4096, 2048], P(('ep', 'tp'))
Inputs may be any that keep to these rules, and one draw needn't show every extreme that they name: `route_ids`: each row names 2 different experts. Within the rows of one device (128 aligned rows) no expert is named more than 40 times, a bound that some block reaches. `query_gain`: Positive.
All inputs are finite; a program needn't handle non-finite values.
Results may differ from a plain program's by a relative error of at most 0.018.
The roundings to bfloat16 on the way count: a program that leaves them out, or rounds other values in their place, can miss the bound.
Values may be sent and summed in bfloat16 or wider, within the bound.
No kernel may reach another device: no remote copies, remote signals or barrier semaphores. Data moves between devices by JAX's collectives and lax.ppermute only.
A program may use at most 128 MiB of HBM per device.

v0:
```python
import math

import jax
import jax.numpy as jnp
from jax import lax
from jax.sharding import PartitionSpec as P

NOPE = 64
ROPE = 32
VDIM = 64


EPS = 1e-06
CLAMP = 7.0
ALPHA = 1.702
THETA = 10000.0
FLOOR = -1e30


def norm_rows(values, gain):
    values = values.astype(jnp.float32)
    scale = lax.rsqrt(jnp.mean(values * values, axis=-1, keepdims=True) + EPS)
    return values * scale * gain


def turn_tables(positions, width):
    half = width // 2
    freqs = THETA ** (-2.0 * jnp.arange(half, dtype=jnp.float32) / width)
    angles = positions.astype(jnp.float32)[:, None] * freqs[None, :]
    return (jnp.cos(angles), jnp.sin(angles))


def rotate(values, cosine, sine):
    half = values.shape[-1] // 2
    first = values[..., :half]
    second = values[..., half:]
    return jnp.concatenate(
        [first * cosine - second * sine, second * cosine + first * sine], axis=-1
    )


def on_device(
    mixer_input,
    expert_input,
    mixer_gain,
    query_down,
    latent_down,
    rotary_down,
    query_gain,
    latent_gain,
    query_plain,
    query_rotary,
    key_plain,
    value_up,
    output_proj,
    mixed_gain,
    expert_norm,
    route_ids,
    route_weight,
    gate_proj,
    up_proj,
    down_proj,
    expert_gain,
):
    tok_rows = mixer_input.shape[0]
    groups = lax.axis_size("tp")
    group_base = lax.axis_index("ep") * groups * tok_rows
    offset = group_base + lax.axis_index("tp") * tok_rows
    heads_here = query_plain.shape[1] // NOPE
    hidden = norm_rows(mixer_input, mixer_gain).astype(jnp.bfloat16)
    query_lat = norm_rows(
        jnp.dot(hidden, query_down, preferred_element_type=jnp.float32), query_gain
    ).astype(jnp.bfloat16)
    key_lat = norm_rows(
        jnp.dot(hidden, latent_down, preferred_element_type=jnp.float32), latent_gain
    ).astype(jnp.bfloat16)
    cosine, sine = turn_tables(offset + jnp.arange(tok_rows, dtype=jnp.int32), ROPE)
    key_turn = rotate(
        jnp.dot(hidden, rotary_down, preferred_element_type=jnp.float32), cosine, sine
    ).astype(jnp.bfloat16)

    def project_keys(latents):
        keys = jnp.dot(latents, key_plain, preferred_element_type=jnp.float32).astype(jnp.bfloat16)
        values = jnp.dot(latents, value_up, preferred_element_type=jnp.float32).astype(jnp.bfloat16)
        return (keys, values)

    query_rows_all = groups * tok_rows
    scale = (NOPE + ROPE) ** (-0.5)

    def attend_block(carry, keys, values, turned, query_nope, query_pe):
        peak, total, accum = carry
        count = keys.shape[0]
        keys = keys.reshape(count, heads_here, NOPE)
        values = values.reshape(count, heads_here, VDIM)
        scores = jnp.einsum("qhd,khd->qhk", query_nope, keys, preferred_element_type=jnp.float32)
        scores = (
            scores + jnp.einsum("qhr,kr->qhk", query_pe, turned, preferred_element_type=jnp.float32)
        ) * scale
        new_peak = jnp.maximum(peak, jnp.max(scores, axis=-1))
        expos = jnp.exp(scores - new_peak[..., None])
        shrink = jnp.exp(peak - new_peak)
        total = total * shrink + jnp.sum(expos, axis=-1)
        accum = accum * shrink[..., None] + jnp.einsum(
            "qhk,khd->qhd", expos.astype(jnp.bfloat16), values, preferred_element_type=jnp.float32
        )
        return (new_peak, total, accum)

    start_state = (
        jnp.full((query_rows_all, heads_here), FLOOR, jnp.float32),
        jnp.zeros((query_rows_all, heads_here), jnp.float32),
        jnp.zeros((query_rows_all, heads_here, VDIM), jnp.float32),
    )
    piece = lax.all_gather(query_lat, "tp", axis=0, tiled=True)
    count = piece.shape[0]
    plain = jnp.dot(piece, query_plain, preferred_element_type=jnp.float32).astype(jnp.bfloat16)
    piece_cos, piece_sin = turn_tables(group_base + jnp.arange(count, dtype=jnp.int32), ROPE)
    rotated = jnp.dot(piece, query_rotary, preferred_element_type=jnp.float32).reshape(
        count, heads_here, ROPE
    )
    rotated = rotate(rotated, piece_cos[:, None, :], piece_sin[:, None, :]).astype(jnp.bfloat16)
    query_all = jnp.concatenate([plain, rotated.reshape(count, heads_here * ROPE)], axis=1)
    carry = start_state
    piece = (
        lax.all_gather(key_lat, ("ep", "tp"), axis=0, tiled=True),
        lax.all_gather(key_turn, ("ep", "tp"), axis=0, tiled=True),
    )
    query_nope = query_all[:, : heads_here * NOPE].reshape(query_rows_all, heads_here, NOPE)
    query_pe = query_all[:, heads_here * NOPE :].reshape(query_rows_all, heads_here, ROPE)
    count = piece[0].shape[0]
    size = math.gcd(count, 1024)
    blocked = tuple((item.reshape(count // size, size, item.shape[1]) for item in piece))

    def step(inner, members):
        keys, values = project_keys(members[0])
        turned = members[1]
        return (attend_block(inner, keys, values, turned, query_nope, query_pe), None)

    carry, _ = lax.scan(step, carry, blocked)
    attended = (
        (carry[2] / carry[1][..., None])
        .astype(jnp.bfloat16)
        .reshape(query_rows_all, heads_here * VDIM)
    )
    rows = attended
    mixed = lax.psum_scatter(
        jnp.dot(rows, output_proj, preferred_element_type=jnp.float32).astype(jnp.bfloat16),
        "tp",
        scatter_dimension=0,
        tiled=True,
    ).astype(jnp.float32)
    mixer_out = norm_rows(mixed, mixed_gain).astype(jnp.bfloat16)
    expert_hidden = norm_rows(expert_input, expert_norm).astype(jnp.bfloat16)
    experts = lax.axis_size("ep")
    topk = route_ids.shape[1]
    capacity = 5 * tok_rows * topk // (4 * experts)
    slots = experts * capacity
    flat_ids = route_ids.reshape(-1)
    onehot = (flat_ids[:, None] == jnp.arange(experts, dtype=jnp.int32)[None, :]).astype(jnp.int32)
    order = jnp.sum((jnp.cumsum(onehot, axis=0) - onehot) * onehot, axis=1)
    target = flat_ids * capacity + order
    dispatch = jnp.any(
        target.reshape(tok_rows, topk)[None, :, :]
        == jnp.arange(slots, dtype=jnp.int32)[:, None, None],
        axis=2,
    ).astype(jnp.bfloat16)
    outgoing = (
        jnp.dot(dispatch, expert_hidden, preferred_element_type=jnp.float32)
        .astype(jnp.bfloat16)
        .reshape(experts, capacity, expert_hidden.shape[1])
    )
    gate_w = gate_proj[0]
    up_w = up_proj[0]
    down_w = down_proj[0]
    received = lax.all_to_all(outgoing, "ep", split_axis=0, concat_axis=0, tiled=True)
    sources, count, width = received.shape
    rows = received.reshape(sources * count, width)
    piece = lax.all_gather(rows, "tp", axis=0, tiled=True)
    gate = jnp.minimum(jnp.dot(piece, gate_w, preferred_element_type=jnp.float32), CLAMP)
    up = jnp.clip(jnp.dot(piece, up_w, preferred_element_type=jnp.float32), -CLAMP, CLAMP)
    acts = ((up + 1.0) * gate * jax.nn.sigmoid(ALPHA * gate)).astype(jnp.bfloat16)
    sums = lax.psum_scatter(
        jnp.dot(acts, down_w, preferred_element_type=jnp.float32).astype(jnp.bfloat16),
        "tp",
        scatter_dimension=0,
        tiled=True,
    )
    returned = sums.reshape(sources, count, width)
    back_rows = lax.all_to_all(returned, "ep", split_axis=0, concat_axis=0, tiled=True).reshape(
        slots, expert_hidden.shape[1]
    )
    picked = back_rows[target].astype(jnp.float32).reshape(tok_rows, topk, expert_hidden.shape[1])
    combined = jnp.sum(picked * route_weight[:, :, None], axis=1)
    expert_out = norm_rows(combined, expert_gain).astype(jnp.bfloat16)
    return (mixer_out, expert_out)


def solution(mesh):
    in_specs = (
        P(("ep", "tp"), None),
        P(("ep", "tp"), None),
        P(),
        P(),
        P(),
        P(),
        P(),
        P(),
        P(None, "tp"),
        P(None, "tp"),
        P(None, "tp"),
        P(None, "tp"),
        P("tp", None),
        P(),
        P(),
        P(("ep", "tp"), None),
        P(("ep", "tp"), None),
        P("ep", None, "tp"),
        P("ep", None, "tp"),
        P("ep", "tp", None),
        P(),
    )
    out_specs = (P(("ep", "tp"), None), P(("ep", "tp"), None))
    return jax.shard_map(
        on_device, mesh=mesh, in_specs=in_specs, out_specs=out_specs, check_vma=False
    )
```

profile of v0, /device:TPU:0, one launch (start us, length us, event | category | flops | bytes accessed | tf_op | source)
XLA Modules:
  0.0 282.0 jit_solution(6880565133789044939)
XLA Ops:
  7.2 1.4 fusion.29
  8.6 4.1 %multiply_reduce_fusion.2 = (f32[128]{0:T(128)S(1)}, f32[128,1536]{1,0:T(8,128)S(1)}) fusion(bf16[2048,1536]{1,0:T(8,128)(2,1)} %param.26, bf16[128,2048]{1,0:T(8,128)(2,1)} %param.23, f32[2048]{0:T(1024)} %param.25, f32[128]{0:T(128)S(1)} %add_rsqrt_fusion.5), kind=kOutput, calls=%fused_computation.58 | convolution fusion | flops 806748032 | bytes 7611392 | tf_op jit(solution)/shard_map/dot_general | solution.py:72
  12.8 0.9 multiply_convert_fusion.1
  13.7 0.1 copy.35
  13.9 0.1 eq.42
  14.0 0.1 eq.38
  14.1 0.6 reduce-window.6
  14.7 0.2 slice_reduce_fusion
  15.0 0.1 fusion.53
  15.1 0.1 reduce_sum.90
  15.3 0.1 copy.38
  15.4 0.2 fusion.35
  15.6 0.6 convolution_convert_fusion.4
  16.2 38.6 %all_to_all.10 = bf16[8,40,2048]{2,1,0:T(8,128)(2,1)} all-to-all(bf16[8,40,2048]{2,1,0:T(8,128)(2,1)S(1)} %bitcast.104), channel_id=1, replica_groups=mesh['ep'=8,'tp'=4] {'ep'}, dimensions={0} | all-to-all | bytes 2621440 | tf_op jit(solution)/shard_map/all_to_all | solution.py:174
  54.9 2.2 multiply_reduce_fusion.3
  57.1 0.7 multiply_convert_fusion.2
  58.0 0.4 fusion.60
  58.3 0.1 fusion.49
  58.5 41.0 %all_gather.14 = bf16[4096,32]{0,1:T(8,128)(2,1)S(1)} all-gather(bf16[128,32]{0,1:T(8,128)(2,1)S(1)} %pad_maximum_fusion.1), channel_id=1, replica_groups=mesh['ep'=8,'tp'=4] {'ep','tp'}, dimensions={0}, use_global_device_ids=true | all-gather | bytes 270336 | tf_op jit(solution)/shard_map/all_gather | solution.py:125
  99.5 0.2 multiply_cosine_fusion
  99.7 2.3 fusion.68
  102.1 0.6 convolution_convert_fusion.5
  102.7 7.5 %convolution_minimum_fusion = f32[1280,512]{1,0:T(8,128)} fusion(bf16[1280,2048]{1,0:T(8,128)(2,1)} %all-gather.8.cloned.1.call-done, bf16[1,2048,512]{2,1,0:T(8,128)(2,1)} %param.40), kind=kOutput, calls=%fused_computation.28 | convolution fusion | flops 2685009920 | bytes 9961472 | tf_op jit(solution)/shard_map/dot_general | solution.py:178
  110.3 10.5 %convolution_convert_fusion.2 = bf16[1280,2048]{1,0:T(8,128)(2,1)} fusion(bf16[1,512,2048]{2,1,0:T(8,128)(2,1)S(1)} %copy-done, f32[1280,512]{1,0:T(8,128)} %convolution_minimum_fusion, bf16[1280,2048]{1,0:T(8,128)(2,1)} %all-gather.8.cloned.1.call-done, bf16[1,2048,512]{2,1,0:T(8,128)(2,1)} %param.41), kind=kOutput, calls=%fused_computation.26 | convolution fusion | flops 5377228800 | bytes 17301504 | tf_op jit(solution)/shard_map/dot_general | solution.py:182
  120.8 0.2 reduce-scatter.3.cloned.1.call-start
  121.0 40.8 %all-gather.4.cloned.1.call-done = bf16[4096,512]{1,0:T(8,128)(2,1)} async-done(((bf16[128,512]{1,0:T(8,128)(2,1)}), bf16[4096,512]{1,0:T(8,128)(2,1)}) %all-gather.4.cloned.1.call-update) | async-done | bytes 4194320 | tf_op jit(solution)/shard_map/all_gather | solution.py:124
  161.8 64.6 %while.15 = (s32[]{:T(128)}, f32[512,4]{0,1:T(4,128)S(1)}, f32[512,4]{0,1:T(4,128)S(1)}, f32[512,4,64]{0,2,1:T(8,128)S(1)}, bf16[4,1024,512]{2,1,0:T(8,128)(2,1)...) while((s32[]{:T(128)}, f32[512,4]{0,1:T(4,128)S(1)}, ...), condition=%wide.region_6.7_spmd.clone, body=%wide.region_3.6_spmd.clone.sunk | while | flops 1223567360 | bytes 81855640 | solution.py:138
  161.8 1.7 convolution_convert_fusion.8
  163.5 1.3 fusion.110
  164.8 4.9 %fusion.111 = (f32[512,4]{0,1:T(4,128)S(1)}, f32[512,4,1024]{0,2,1:T(8,128)}) fusion(bf16[512,4,32]{0,2,1:T(8,128)(2,1)S(1)} %get-tuple-element.257, bf16[4,1024,32]{1,2,0:T(8,128)(2,1)S(1)} %get-tuple-element.256, s32[]{:T(128)} %get-tuple-element.237, f32[4,1024,512]{2,1,0:T(8,128)S(1)} %fusion.110), kind=kOutput, calls=%fused_computation.110.clone.1 | convolution fusion | flops 140507136 | bytes 16982020 | tf_op jit(solution)/shard_map/while/body/eval_jaxpr/qhr,kr->qhk/dot_general | solution.py:97
  169.8 6.2 %fusion.112 = f32[512,4]{0,1:T(4,128)S(1)} fusion(f32[512,4,1024]{0,2,1:T(8,128)} %get-tuple-element.222, f32[512,4]{0,1:T(4,128)S(1)} %select_maximum_fusion.2), kind=kLoop, calls=%fused_computation.5.clone.1 | loop fusion | flops 4192256 | bytes 8404992 | tf_op jit(solution)/shard_map/while/body/eval_jaxpr/reduce_sum | solution.py:102
  176.0 2.0 convolution_convert_fusion.9
  178.0 1.5 fusion.114
  179.6 1.7 convolution_convert_fusion.8
  181.3 1.3 fusion.110
  182.6 4.5 %fusion.111 = (f32[512,4]{0,1:T(4,128)S(1)}, f32[512,4,1024]{0,2,1:T(8,128)}) fusion(bf16[512,4,32]{0,2,1:T(8,128)(2,1)S(1)} %get-tuple-element.257, bf16[4,1024,32]{1,2,0:T(8,128)(2,1)S(1)} %get-tuple-element.256, s32[]{:T(128)} %get-tuple-element.237, f32[4,1024,512]{2,1,0:T(8,128)S(1)} %fusion.110), kind=kOutput, calls=%fused_computation.110.clone.1 | convolution fusion | flops 140507136 | bytes 16982020 | tf_op jit(solution)/shard_map/while/body/eval_jaxpr/qhr,kr->qhk/dot_general | solution.py:97
  187.1 4.7 %fusion.112 = f32[512,4]{0,1:T(4,128)S(1)} fusion(f32[512,4,1024]{0,2,1:T(8,128)} %get-tuple-element.222, f32[512,4]{0,1:T(4,128)S(1)} %select_maximum_fusion.2), kind=kLoop, calls=%fused_computation.5.clone.1 | loop fusion | flops 4192256 | bytes 8404992 | tf_op jit(solution)/shard_map/while/body/eval_jaxpr/reduce_sum | solution.py:102
  191.9 1.7 convolution_convert_fusion.9
  193.6 1.5 fusion.114
  195.2 1.7 convolution_convert_fusion.8
  196.9 1.3 fusion.110
  198.2 4.5 %fusion.111 = (f32[512,4]{0,1:T(4,128)S(1)}, f32[512,4,1024]{0,2,1:T(8,128)}) fusion(bf16[512,4,32]{0,2,1:T(8,128)(2,1)S(1)} %get-tuple-element.257, bf16[4,1024,32]{1,2,0:T(8,128)(2,1)S(1)} %get-tuple-element.256, s32[]{:T(128)} %get-tuple-element.237, f32[4,1024,512]{2,1,0:T(8,128)S(1)} %fusion.110), kind=kOutput, calls=%fused_computation.110.clone.1 | convolution fusion | flops 140507136 | bytes 16982020 | tf_op jit(solution)/shard_map/while/body/eval_jaxpr/qhr,kr->qhk/dot_general | solution.py:97
  202.7 4.7 %fusion.112 = f32[512,4]{0,1:T(4,128)S(1)} fusion(f32[512,4,1024]{0,2,1:T(8,128)} %get-tuple-element.222, f32[512,4]{0,1:T(4,128)S(1)} %select_maximum_fusion.2), kind=kLoop, calls=%fused_computation.5.clone.1 | loop fusion | flops 4192256 | bytes 8404992 | tf_op jit(solution)/shard_map/while/body/eval_jaxpr/reduce_sum | solution.py:102
  207.4 1.9 convolution_convert_fusion.9
  209.3 1.5 fusion.114
  210.9 1.7 convolution_convert_fusion.8
  212.6 1.3 fusion.110
  213.9 4.5 %fusion.111 = (f32[512,4]{0,1:T(4,128)S(1)}, f32[512,4,1024]{0,2,1:T(8,128)}) fusion(bf16[512,4,32]{0,2,1:T(8,128)(2,1)S(1)} %get-tuple-element.257, bf16[4,1024,32]{1,2,0:T(8,128)(2,1)S(1)} %get-tuple-element.256, s32[]{:T(128)} %get-tuple-element.237, f32[4,1024,512]{2,1,0:T(8,128)S(1)} %fusion.110), kind=kOutput, calls=%fused_computation.110.clone.1 | convolution fusion | flops 140507136 | bytes 16982020 | tf_op jit(solution)/shard_map/while/body/eval_jaxpr/qhr,kr->qhk/dot_general | solution.py:97
  218.4 4.7 %fusion.112 = f32[512,4]{0,1:T(4,128)S(1)} fusion(f32[512,4,1024]{0,2,1:T(8,128)} %get-tuple-element.222, f32[512,4]{0,1:T(4,128)S(1)} %select_maximum_fusion.2), kind=kLoop, calls=%fused_computation.5.clone.1 | loop fusion | flops 4192256 | bytes 8404992 | tf_op jit(solution)/shard_map/while/body/eval_jaxpr/reduce_sum | solution.py:102
  223.1 1.7 convolution_convert_fusion.9
  224.9 1.5 fusion.114
  226.5 3.3 %convolution_convert_fusion.3 = bf16[512,2048]{1,0:T(8,128)(2,1)} fusion(bf16[512,256]{0,1:T(8,128)(2,1)S(1)} %bitcast.105, bf16[256,2048]{1,0:T(8,128)(2,1)} %param.35), kind=kOutput, calls=%fused_computation.32 | convolution fusion | flops 537919488 | bytes 3407872 | tf_op jit(solution)/shard_map/dot_general | solution.py:146
  229.9 4.1 %all-to-all-start.1 = ((bf16[8,40,2048]{2,1,0:T(8,128)(2,1)}), bf16[8,40,2048]{2,1,0:T(8,128)(2,1)S(1)}, u32[]{:S(2)}, u32[]{:S(2)}) async-start(bf16[8,40,2048]{2,1,0:T(8,128)(2,1)} %bitcast.107), calls=%async_computation.3 | async-start | bytes 2621440 | tf_op jit(solution)/shard_map/all_to_all | solution.py:188
  234.0 0.1 mul.302
  234.1 0.1 copy.39
  234.3 25.9 %reduce-scatter.3.cloned.1.call-done = bf16[128,2048]{1,0:T(8,128)(2,1)} async-done(((bf16[512,2048]{1,0:T(8,128)(2,1)}), bf16[128,2048]{1,0:T(8,128)(2,1)}) %reduce-scatter.3.cloned.1.call-update) | async-done | bytes 524304 | tf_op jit(solution)/shard_map/reduce_scatter | solution.py:145
  260.2 1.2 fusion.32
  261.4 2.0 fusion.34
  263.4 2.4 all-to-all-done.1
  265.8 1.4 gather_fusion
  267.2 2.4 reshape.223
  269.6 4.8 %multiply_reduce_fusion = f32[128,2048]{1,0:T(8,128)S(1)} fusion(f32[128,2,2048]{2,1,0:T(2,128)} %reshape.223, f32[128,2]{1,0:T(8,128)S(1)} %copy.39), kind=kLoop, calls=%fused_computation.38 | loop fusion | flops 786432 | bytes 3146752 | tf_op jit(solution)/shard_map/reduce_sum | solution.py:192
  274.4 0.2 multiply_reduce_fusion.1
  274.6 1.0 multiply_convert_fusion
  (90 shorter events, 0.9 us)
Async XLA Ops:
  7.2 103.1 %copy-start = (bf16[1,512,2048]{2,1,0:T(8,128)(2,1)S(1)}, bf16[1,512,2048]{2,1,0:T(8,128)(2,1)}, u32[]{:S(2)}) copy-start(bf16[1,512,2048]{2,1,0:T(8,128)(2,1)} %param.42) | copy-start | bytes 6291460
  7.2 92.5 %all-gather.6.cloned.1.call-start = ((), (), s32[]{:S(2)}) async-start(), calls=%async_computation.5 | async-start | bytes 1966080 | tf_op jit(solution)/shard_map/all_gather | solution.py:113
  8.6 4.2 %copy-start.8 = (f32[1536]{0:T(1024)S(1)}, f32[1536]{0:T(1024)}, u32[]{:S(2)}) copy-start(f32[1536]{0:T(1024)} %param.29) | copy-start | bytes 18436
  8.6 5.1 %copy-start.14 = (s32[128,2]{0,1:T(2,128)S(1)}, s32[128,2]{0,1:T(2,128)}, u32[]{:S(2)}) copy-start(s32[128,2]{0,1:T(2,128)} %param.38) | copy-start | bytes 3076
  12.7 2.7 copy-start.6
  12.7 2.9 %copy-start.9 = (f32[2048]{0:T(1024)S(1)}, f32[2048]{0:T(1024)}, u32[]{:S(2)}) copy-start(f32[2048]{0:T(1024)} %param.37) | copy-start | bytes 24580
  13.7 89.0 %all-gather.8.cloned.1.call-start = ((), (), s32[]{:S(2)}) async-start(), calls=%async_computation.7 | async-start | bytes 6553600 | tf_op jit(solution)/shard_map/all_gather | solution.py:177
  15.6 39.3 %copy-start.5 = (bf16[128,2048]{1,0:T(8,128)(2,1)S(1)}, bf16[128,2048]{1,0:T(8,128)(2,1)}, u32[]{:S(2)}) copy-start(bf16[128,2048]{1,0:T(8,128)(2,1)} %param.23) | copy-start | bytes 1572868
  15.6 39.3 %copy-start.10 = (f32[2048]{0:T(1024)S(1)}, f32[2048]{0:T(1024)}, u32[]{:S(2)}) copy-start(f32[2048]{0:T(1024)} %param.25) | copy-start | bytes 24580
  54.8 2.3 copy-start.13
  54.8 3.2 %copy-start.17 = (bf16[2048,32]{0,1:T(8,128)(2,1)S(1)}, bf16[2048,32]{0,1:T(8,128)(2,1)}, u32[]{:S(2)}) copy-start(bf16[2048,32]{0,1:T(8,128)(2,1)} %param.28) | copy-start | bytes 393220
  54.8 107.0 %all-gather.4.cloned.1.call-start = ((), (), s32[]{:S(2)}) async-start(), calls=%async_computation.4 | async-start | bytes 4325376 | tf_op jit(solution)/shard_map/all_gather | solution.py:124
  57.9 172.0 %reduce-scatter.5.cloned.1.call-start = ((), (), s32[]{:S(2)}) async-start(), calls=%async_computation.8 | async-start | bytes 6553600 | tf_op jit(solution)/shard_map/reduce_scatter | solution.py:181
  99.7 2.4 copy-start.7
  99.7 2.4 copy-start.16
  120.8 41.0 %copy-start.3 = (bf16[512,256]{1,0:T(8,128)(2,1)S(1)}, bf16[512,256]{1,0:T(8,128)(2,1)}, u32[]{:S(2)}) copy-start(bf16[512,256]{1,0:T(8,128)(2,1)} %param.33) | copy-start | bytes 786436
  120.8 41.0 %copy-start.4 = (bf16[512,256]{1,0:T(8,128)(2,1)S(1)}, bf16[512,256]{1,0:T(8,128)(2,1)}, u32[]{:S(2)}) copy-start(bf16[512,256]{1,0:T(8,128)(2,1)} %param.34) | copy-start | bytes 786436
  120.8 139.4 %reduce-scatter.3.cloned.1.call-start = ((), (), s32[]{:S(2)}) async-start(), calls=%async_computation.6 | async-start | bytes 2621440 | tf_op jit(solution)/shard_map/reduce_scatter | solution.py:145
  169.8 8.3 %copy-start.2 = (f32[512,4,1024]{0,2,1:T(8,128)S(1)}, f32[512,4,1024]{0,2,1:T(8,128)}, u32[]{:S(2)}) copy-start(f32[512,4,1024]{0,2,1:T(8,128)} %get-tuple-element.222) | copy-start | bytes 25165828 | tf_op jit(solution)/shard_map/while
  187.1 6.5 %copy-start.2 = (f32[512,4,1024]{0,2,1:T(8,128)S(1)}, f32[512,4,1024]{0,2,1:T(8,128)}, u32[]{:S(2)}) copy-start(f32[512,4,1024]{0,2,1:T(8,128)} %get-tuple-element.222) | copy-start | bytes 25165828 | tf_op jit(solution)/shard_map/while
  202.7 6.6 %copy-start.2 = (f32[512,4,1024]{0,2,1:T(8,128)S(1)}, f32[512,4,1024]{0,2,1:T(8,128)}, u32[]{:S(2)}) copy-start(f32[512,4,1024]{0,2,1:T(8,128)} %get-tuple-element.222) | copy-start | bytes 25165828 | tf_op jit(solution)/shard_map/while
  218.4 6.5 %copy-start.2 = (f32[512,4,1024]{0,2,1:T(8,128)S(1)}, f32[512,4,1024]{0,2,1:T(8,128)}, u32[]{:S(2)}) copy-start(f32[512,4,1024]{0,2,1:T(8,128)} %get-tuple-element.222) | copy-start | bytes 25165828 | tf_op jit(solution)/shard_map/while
  229.8 4.3 %copy-start.15 = (f32[128,2]{0,1:T(2,128)S(1)}, f32[128,2]{0,1:T(2,128)}, u32[]{:S(2)}) copy-start(f32[128,2]{0,1:T(2,128)} %param.39) | copy-start | bytes 3076
  229.8 31.6 %copy-start.11 = (f32[2048]{0:T(1024)S(1)}, f32[2048]{0:T(1024)}, u32[]{:S(2)}) copy-start(f32[2048]{0:T(1024)} %param.36) | copy-start | bytes 24580
  229.9 36.0 %all-to-all-start.1 = ((bf16[8,40,2048]{2,1,0:T(8,128)(2,1)}), bf16[8,40,2048]{2,1,0:T(8,128)(2,1)S(1)}, u32[]{:S(2)}, u32[]{:S(2)}) async-start(bf16[8,40,2048]{2,1,0:T(8,128)(2,1)} %bitcast.107), calls=%async_computation.3 | async-start | bytes 2621440 | tf_op jit(solution)/shard_map/all_to_all | solution.py:188
  267.2 8.3 %copy-start.1 = (bf16[1,512,2048]{2,1,0:T(8,128)(2,1)S(1)}, bf16[1,512,2048]{2,1,0:T(8,128)(2,1)}, u32[]{:S(2)}) copy-start(bf16[1,512,2048]{2,1,0:T(8,128)(2,1)} %param.42) | copy-start | bytes 6291460
  269.6 5.0 %copy-start.12 = (f32[2048]{0:T(1024)S(1)}, f32[2048]{0:T(1024)}, u32[]{:S(2)}) copy-start(f32[2048]{0:T(1024)} %param.43) | copy-start | bytes 24580
Sparse Core Ops, SparseCore 0:
  13.8 22.3 all-gather.5
  54.9 41.5 all-gather.7
  100.0 61.7 all-gather.3
  164.2 50.1 reduce-scatter.4
  230.0 30.1 reduce-scatter.2
where the time goes:
time: 283 us; the launch traced here: 282 us
  blocking collectives  79.5 us (28%)
  matrix products  75.3 us (27%)
  waiting for transfers between devices  69.2 us (24%)
  other arithmetic  34.1 us (12%)
  between operations  14.2 us (5%)
  local copies, waits for them, and re-layouts  4.93 us (2%)
  starting transfers between devices  4.52 us (2%)
    all_gather x1, blocking collectives, on_device(): lax.all_gather(key_turn, ('ep', 'tp'), axis=0, tiled=True)  41 us
    all_gather x1, waiting for transfers between devices, on_device(): lax.all_gather(key_lat, ('ep', 'tp'), axis=0, tiled=True)  40.8 us
    all_to_all x1, blocking collectives, on_device(): lax.all_to_all(outgoing, 'ep', split_axis=0, concat_axis=0, tiled=True)  38.6 us
    reduce_scatter x1, waiting for transfers between devices, on_device(): lax.psum_scatter(jnp.dot(rows, output_proj, preferred_element_type=jnp.fl...  25.9 us
    reduce_sum x4, other arithmetic, attend_block(): total = total * shrink + jnp.sum(expos, axis=-1)  20.3 us
    dot_general x4, matrix products, attend_block(): jnp.einsum('qhr,kr->qhk', query_pe, turned, preferred_element_type=jnp.fl...  18.5 us
    dot_general x1, matrix products, on_device(): jnp.dot(acts, down_w, preferred_element_type=jnp.float32)  10.5 us
    dot_general x1, matrix products, on_device(): jnp.dot(piece, gate_w, preferred_element_type=jnp.float32)  7.55 us
  transfers between devices with their start and end apart: 6, of which 3 were waited for; matrix products, arithmetic and copies ran while one was open for 35% of the time, Pallas kernels for 0%

commit v1 on v0

v1 whole, which is shorter than its diff:
```python
import math

import jax
import jax.numpy as jnp
from jax import lax
from jax.experimental import pallas as pl
from jax.experimental.pallas import tpu as pltpu
from jax.sharding import PartitionSpec as P

NOPE = 64
ROPE = 32
VDIM = 64


EPS = 1e-06
CLAMP = 7.0
ALPHA = 1.702
THETA = 10000.0
LOG2E = math.log2(math.e)


def norm_rows(values, gain):
    values = values.astype(jnp.float32)
    scale = lax.rsqrt(jnp.mean(values * values, axis=-1, keepdims=True) + EPS)
    return values * scale * gain


def turn_tables(positions, width):
    half = width // 2
    freqs = THETA ** (-2.0 * jnp.arange(half, dtype=jnp.float32) / width)
    angles = positions.astype(jnp.float32)[:, None] * freqs[None, :]
    return (jnp.cos(angles), jnp.sin(angles))


def swap_with(values, axis, stride):
    count = lax.axis_size(axis)
    return lax.ppermute(values, axis, [(i, i ^ stride) for i in range(count)])


def shift_by(values, axis, step):
    count = lax.axis_size(axis)
    return lax.ppermute(values, axis, [(i, (i + step) % count) for i in range(count)])


def strides_of(axis):
    count = lax.axis_size(axis)
    return [1 << b for b in reversed(range(count.bit_length() - 1))]


def block_owners(axis):
    owners = [0]
    for stride in strides_of(axis):
        owners = owners + [o ^ stride for o in owners]
    return owners


def gather_rows(values, axis):
    for stride in strides_of(axis):
        values = jnp.concatenate([values, swap_with(values, axis, stride)], axis=0)
    return values


def scatter_sum(values, axis):
    for stride in reversed(strides_of(axis)):
        half = values.shape[0] // 2
        other = swap_with(values[half:], axis, stride)
        values = (values[:half].astype(jnp.float32) + other.astype(jnp.float32)).astype(
            values.dtype
        )
    return values


def attend_kernel(heads, scale, q_block, k_block, qn, qp, lat, wk, wv, out, keys, vals, sc, acc):
    rank = wk.shape[0]
    total = lat.shape[0]
    chunks = total // k_block
    half = lax.broadcasted_iota(jnp.int32, (q_block, 2 * NOPE), 1) // NOPE
    part = lax.broadcasted_iota(jnp.int32, (q_block, heads * ROPE), 1) // ROPE

    def project(c, _):
        at = pl.ds(pl.multiple_of(c * k_block, k_block), k_block)
        rows = lat[at, :rank]
        keys[at, :] = jnp.dot(rows, wk[...], preferred_element_type=jnp.float32).astype(keys.dtype)
        vals[at, :] = jnp.dot(rows, wv[...], preferred_element_type=jnp.float32).astype(vals.dtype)
        return 0

    lax.fori_loop(0, chunks, project, 0)

    def one_block(b, _):
        rows = pl.ds(pl.multiple_of(b * q_block, q_block), q_block)
        for pair in range(heads // 2):
            cols = slice(pair * 2 * NOPE, (pair + 1) * 2 * NOPE)
            done = []
            for side in range(2):
                plain = qn[rows, cols]
                plain = jnp.where(half == side, plain, jnp.zeros_like(plain))
                turned = qp[rows, :]
                turned = jnp.where(part == 2 * pair + side, turned, jnp.zeros_like(turned))
                query = jnp.concatenate([plain, turned], axis=1)

                def score(c, peak):
                    at = pl.ds(pl.multiple_of(c * k_block, k_block), k_block)
                    block = jnp.concatenate([keys[at, cols], lat[at, rank:]], axis=1)
                    s = lax.dot_general(
                        query, block, (((1,), (1,)), ((), ())), preferred_element_type=jnp.float32
                    )
                    sc[c] = s
                    for j in range(k_block // 128):
                        peak = jnp.maximum(peak, s[:, j * 128 : (j + 1) * 128])
                    return peak

                peak = lax.fori_loop(
                    0, chunks, score, jnp.full((q_block, 128), -jnp.inf, jnp.float32)
                )
                peak = jnp.max(peak, axis=1, keepdims=True) * (scale * LOG2E)
                acc[...] = jnp.zeros_like(acc)

                def blend(c, _):
                    at = pl.ds(pl.multiple_of(c * k_block, k_block), k_block)
                    w = jnp.exp2(sc[c] * (scale * LOG2E) - peak).astype(jnp.bfloat16)
                    v = vals[at, cols]
                    v = jnp.concatenate([v, jnp.ones_like(v)], axis=1)
                    acc[...] += jnp.dot(w, v, preferred_element_type=jnp.float32)
                    return 0

                lax.fori_loop(0, chunks, blend, 0)
                done.append(acc[:, : 2 * VDIM] / acc[:, 2 * VDIM :])
            out[rows, cols] = jnp.where(half == 0, done[0], done[1]).astype(out.dtype)
        return 0

    lax.fori_loop(0, qn.shape[0] // q_block, one_block, 0)


def attend(query_nope, query_pe, latents, key_plain, value_up):
    rows, width = query_nope.shape
    total = latents.shape[0]
    heads = width // NOPE
    k_block = math.gcd(total, 1024)
    q_block = math.gcd(rows, max(128, min(512, (1 << 21) // total)))
    vmem = pl.BlockSpec(memory_space=pltpu.VMEM)
    pairs = rows * heads * total

    def body(*refs):
        attend_kernel(heads, (NOPE + ROPE) ** (-0.5), q_block, k_block, *refs)

    return pl.pallas_call(
        body,
        out_shape=jax.ShapeDtypeStruct((rows, heads * VDIM), jnp.bfloat16),
        in_specs=[vmem] * 5,
        out_specs=vmem,
        scratch_shapes=[
            pltpu.VMEM((total, width), jnp.bfloat16),
            pltpu.VMEM((total, width), jnp.bfloat16),
            pltpu.VMEM((total // k_block, q_block, k_block), jnp.float32),
            pltpu.VMEM((q_block, 4 * VDIM), jnp.float32),
        ],
        cost_estimate=pl.CostEstimate(
            flops=pairs * 1024, transcendentals=pairs, bytes_accessed=total * 1280
        ),
        name="attend",
    )(query_nope, query_pe, latents, key_plain, value_up)


def on_device(
    mixer_input,
    expert_input,
    mixer_gain,
    query_down,
    latent_down,
    rotary_down,
    query_gain,
    latent_gain,
    query_plain,
    query_rotary,
    key_plain,
    value_up,
    output_proj,
    mixed_gain,
    expert_norm,
    route_ids,
    route_weight,
    gate_proj,
    up_proj,
    down_proj,
    expert_gain,
):
    tok_rows = mixer_input.shape[0]
    groups = lax.axis_size("tp")
    me_tp = lax.axis_index("tp")
    me_ep = lax.axis_index("ep")
    group_base = me_ep * groups * tok_rows
    heads_here = query_plain.shape[1] // NOPE

    expert_hidden = norm_rows(expert_input, expert_norm).astype(jnp.bfloat16)
    experts = lax.axis_size("ep")
    topk = route_ids.shape[1]
    capacity = 5 * tok_rows * topk // (4 * experts)
    slots = experts * capacity
    flat_ids = route_ids.reshape(-1)
    onehot = (flat_ids[:, None] == jnp.arange(experts, dtype=jnp.int32)[None, :]).astype(jnp.int32)
    order = jnp.sum((jnp.cumsum(onehot, axis=0) - onehot) * onehot, axis=1)
    target = (((flat_ids - me_ep) % experts) * capacity + order).reshape(tok_rows, topk)
    slot_ids = jnp.arange(slots, dtype=jnp.int32)
    dispatch = jnp.any(target[None, :, :] == slot_ids[:, None, None], axis=2).astype(jnp.bfloat16)
    width = expert_hidden.shape[1]
    outgoing = (
        jnp.dot(dispatch, expert_hidden, preferred_element_type=jnp.float32)
        .astype(jnp.bfloat16)
        .reshape(experts, capacity, width)
    )
    halves = [range(0, experts // 2), range(experts // 2, experts)]

    def arrive(members):
        blocks = [outgoing[s] if s == 0 else shift_by(outgoing[s], "ep", s) for s in members]
        return gather_rows(jnp.concatenate(blocks, axis=0), "tp")

    arrived = [arrive(members) for members in halves]

    hidden = norm_rows(mixer_input, mixer_gain).astype(jnp.bfloat16)
    own = jnp.array(block_owners("tp"), jnp.int32) ^ me_tp
    positions = (
        group_base + own[:, None] * tok_rows + jnp.arange(tok_rows, dtype=jnp.int32)[None, :]
    ).reshape(-1)
    cosine, sine = turn_tables(positions, ROPE)
    cosine = jnp.concatenate([cosine] * (2 * heads_here), axis=1)
    sine = jnp.concatenate([sine] * (2 * heads_here), axis=1)

    def swapped(weights):
        rows = weights.shape[0]
        parts = weights.reshape(rows, -1, 2, ROPE // 2)
        return jnp.stack([-parts[:, :, 1], parts[:, :, 0]], axis=2).reshape(weights.shape)

    key_lat = norm_rows(
        jnp.dot(hidden, latent_down, preferred_element_type=jnp.float32), latent_gain
    ).astype(jnp.bfloat16)
    turn_w = jnp.concatenate([rotary_down] * heads_here, axis=1)
    turn_w_swapped = jnp.concatenate([swapped(rotary_down)] * heads_here, axis=1)
    key_turn = (
        jnp.dot(hidden, turn_w, preferred_element_type=jnp.float32) * cosine[:tok_rows]
        + jnp.dot(hidden, turn_w_swapped, preferred_element_type=jnp.float32) * sine[:tok_rows]
    ).astype(jnp.bfloat16)
    latents = lax.all_gather(
        jnp.concatenate([key_lat, key_turn], axis=1), ("ep", "tp"), axis=0, tiled=True
    )
    query_lat = norm_rows(
        jnp.dot(hidden, query_down, preferred_element_type=jnp.float32), query_gain
    ).astype(jnp.bfloat16)
    query_rows = gather_rows(query_lat, "tp")
    query_nope = jnp.dot(query_rows, query_plain, preferred_element_type=jnp.float32).astype(
        jnp.bfloat16
    )
    query_pe = (
        jnp.dot(query_rows, query_rotary, preferred_element_type=jnp.float32) * cosine
        + jnp.dot(query_rows, swapped(query_rotary), preferred_element_type=jnp.float32) * sine
    ).astype(jnp.bfloat16)

    gate_w = gate_proj[0]
    up_w = up_proj[0]
    down_w = down_proj[0]

    def expert_rows(rows):
        gate = jnp.minimum(jnp.dot(rows, gate_w, preferred_element_type=jnp.float32), CLAMP)
        up = jnp.clip(jnp.dot(rows, up_w, preferred_element_type=jnp.float32), -CLAMP, CLAMP)
        acts = ((up + 1.0) * gate * jax.nn.sigmoid(ALPHA * gate)).astype(jnp.bfloat16)
        return jnp.dot(acts, down_w, preferred_element_type=jnp.float32).astype(jnp.bfloat16)

    back = []
    for members, rows in zip(halves, arrived):
        sums = scatter_sum(expert_rows(rows), "tp").reshape(len(members), capacity, width)
        back += [
            sums[i] if s == 0 else shift_by(sums[i], "ep", -s) for i, s in enumerate(members)
        ]

    attended = attend(query_nope, query_pe, latents, key_plain, value_up)
    partial = jnp.dot(attended, output_proj, preferred_element_type=jnp.float32).astype(
        jnp.bfloat16
    )
    mixed = scatter_sum(partial, "tp").astype(jnp.float32)
    mixer_out = norm_rows(mixed, mixed_gain).astype(jnp.bfloat16)

    share = jnp.sum(
        jnp.where(target[:, :, None] == slot_ids[None, None, :], route_weight[:, :, None], 0.0),
        axis=1,
    )
    high = share.astype(jnp.bfloat16)
    low = (share - high.astype(jnp.float32)).astype(jnp.bfloat16)
    back_rows = jnp.concatenate(back, axis=0)
    combined = jnp.dot(high, back_rows, preferred_element_type=jnp.float32) + jnp.dot(
        low, back_rows, preferred_element_type=jnp.float32
    )
    expert_out = norm_rows(combined, expert_gain).astype(jnp.bfloat16)
    return (mixer_out, expert_out)


def solution(mesh):
    in_specs = (
        P(("ep", "tp"), None),
        P(("ep", "tp"), None),
        P(),
        P(),
        P(),
        P(),
        P(),
        P(),
        P(None, "tp"),
        P(None, "tp"),
        P(None, "tp"),
        P(None, "tp"),
        P("tp", None),
        P(),
        P(),
        P(("ep", "tp"), None),
        P(("ep", "tp"), None),
        P("ep", None, "tp"),
        P("ep", None, "tp"),
        P("ep", "tp", None),
        P(),
    )
    out_specs = (P(("ep", "tp"), None), P(("ep", "tp"), None))
    return jax.shard_map(
        on_device, mesh=mesh, in_specs=in_specs, out_specs=out_specs, check_vma=False
    )
```

time: 283 us -> 247 us (0.87)
  blocking collectives: 79.5 us -> 0 us
  starting transfers between devices: 4.52 us -> 45.8 us
  matrix products: 75.3 us -> 37.6 us
  local copies, waits for them, and re-layouts: 4.93 us -> 27.7 us
  Pallas kernels: 0 us -> 22.7 us
  other arithmetic: 34.1 us -> 14.8 us
  waiting for transfers between devices: 69.2 us -> 83.4 us
    ppermute x0 -> x26, waiting for transfers between devices: none -> 83.4 us  [the longest x12 49.8 us: swap_with(): return lax.ppermute(values, axis, [(i, i ^ stride) for i in range(count)])]
    ppermute x0 -> x26, starting transfers between devices: none -> 45.8 us  [the longest x14 37.8 us: shift_by(): lax.ppermute(values, axis, [(i, (i + step) % count) for i in range(count)])]
    all_gather x1 -> x0, blocking collectives: 41 us -> none  [on_device(): lax.all_gather(key_turn, ('ep', 'tp'), axis=0, tiled=True)]
    all_gather x3 -> x1, waiting for transfers between devices: 40.8 us -> 0.02 us  [on_device(): lax.all_gather(jnp.concatenate([key_lat, key_turn], axis=1), ('ep', 'tp')...]
    all_to_all x1 -> x0, blocking collectives: 38.6 us -> none  [on_device(): lax.all_to_all(outgoing, 'ep', split_axis=0, concat_axis=0, tiled=True)]
    dot_general x26 -> x12, matrix products: 68.5 us -> 32.3 us  [the longest x2 14.7 us: expert_rows(): jnp.dot(acts, down_w, preferred_element_type=jnp.float32)]
    reduce_scatter x2 -> x0, waiting for transfers between devices: 25.9 us -> none  [the longest x1 25.9 us: on_device(): lax.psum_scatter(jnp.dot(rows, output_proj, preferred_element_type=jnp.fl...]
    reduce_sum x5 -> x1, other arithmetic: 25.1 us -> 0.04 us  [on_device(): jnp.sum(jnp.where(target[:, :, None] == slot_ids[None, None, :], route_we...]
  transfers between devices with their start and end apart: 6 -> 27, of which waited for: 3 -> 11; matrix products, arithmetic and copies ran while one was open for 35% -> 27% of each run, Pallas kernels for 0% -> 9%
where the time goes in v1:
time: 247 us
  waiting for transfers between devices  83.4 us (34%)
  starting transfers between devices  45.8 us (19%)
  matrix products  37.6 us (15%)
  local copies, waits for them, and re-layouts  27.7 us (11%)
  Pallas kernels  22.7 us (9%)
  other arithmetic  14.8 us (6%)
  between operations  14.7 us (6%)
    ppermute x12, waiting for transfers between devices, swap_with(): return lax.ppermute(values, axis, [(i, i ^ stride) for i in range(count)])  49.8 us
    ppermute x14, starting transfers between devices, shift_by(): lax.ppermute(values, axis, [(i, (i + step) % count) for i in range(count)])  37.8 us
    ppermute x14, waiting for transfers between devices, shift_by(): lax.ppermute(values, axis, [(i, (i + step) % count) for i in range(count)])  33.6 us
    pallas_call x1, Pallas kernels, attend(): pl.pallas_call(body, out_shape=jax.ShapeDtypeStruct((rows, heads * VDIM),...  22.7 us
    unnamed x87, local copies, waits for them, and re-layouts  14.7 us
    dot_general x2, matrix products, expert_rows(): jnp.dot(acts, down_w, preferred_element_type=jnp.float32)  14.7 us
    ppermute x12, starting transfers between devices, swap_with(): return lax.ppermute(values, axis, [(i, i ^ stride) for i in range(count)])  7.95 us
    dot_general x2, matrix products, expert_rows(): jnp.dot(rows, gate_w, preferred_element_type=jnp.float32)  5.18 us
  transfers between devices with their start and end apart: 27, of which 11 were waited for; matrix products, arithmetic and copies ran while one was open for 27% of the time, Pallas kernels for 9%

profile of v1, /device:TPU:0, one launch (start us, length us, event | category | flops | bytes accessed | tf_op | source)
XLA Modules:
  0.0 246.7 jit_solution(12759067061385939425)
XLA Ops:
  7.2 1.4 fusion.50
  8.6 4.1 %multiply_reduce_fusion.1 = (f32[128]{0:T(128)S(1)}, f32[128,1536]{1,0:T(8,128)S(1)}) fusion(bf16[2048,1536]{1,0:T(8,128)(2,1)} %param.25, bf16[128,2048]{1,0:T(8,128)(2,1)} %param.22, f32[2048]{0:T(1024)} %param.24, f32[128]{0:T(128)S(1)} %add_rsqrt_fusion.5), kind=kOutput, calls=%fused_computation.62 | convolution fusion | flops 806748032 | bytes 7611392 | tf_op jit(solution)/shard_map/dot_general | solution.py:246
  12.9 3.0 %collective-permute-start = (bf16[128,1536]{1,0:T(8,128)(2,1)S(1)}, bf16[128,1536]{1,0:T(8,128)(2,1)}, u32[]{:S(2)}, u32[]{:S(2)}) collective-permute-start(bf16[128,1536]{1,0:T(8,128)(2,1)S(1)} %multiply_convert_fusion.1), channel_id=1, source_target_pairs={{0,2},{1,3},{2,0},{3,1},{4,6},{5,7},{6,4},{7,5},{8,10},{9,11},{10,... | collective-permute-start | bytes 1179656 | tf_op jit(solution)/shard_map/ppermute | solution.py:37
  16.0 1.0 multiply_cosine_fusion
  17.0 1.4 concatenate.50
  18.5 0.8 concatenate.49
  19.5 1.6 convolution_multiply_fusion.3
  22.1 1.2 fusion.49
  26.6 1.2 fusion.114
  27.8 1.5 collective-permute-start.4
  29.3 1.6 collective-permute-start.5
  30.9 2.5 %collective-permute-start.6 = (bf16[40,2048]{1,0:T(8,128)(2,1)}, bf16[40,2048]{1,0:T(8,128)(2,1)}, u32[]{:S(2)}, u32[]{:S(2)}) collective-permute-start(bf16[40,2048]{1,0:T(8,128)(2,1)} %get-tuple-element.8), channel_id=1, source_target_pairs={{0,12},{4,16},{8,20},{12,24},{16,28},{20,0},{24,4},{28,8},{1,13},{... | collective-permute-start | bytes 491528 | tf_op jit(solution)/shard_map/ppermute | solution.py:42
  33.4 1.2 collective-permute-start.14
  34.9 0.8 pad_maximum_fusion.4
  35.8 2.3 collective-permute-done.4
  38.5 3.1 %collective-permute-start.16 = (bf16[40,2048]{1,0:T(8,128)(2,1)S(1)}, bf16[40,2048]{1,0:T(8,128)(2,1)S(1)}, u32[]{:S(2)}, u32[]{:S(2)}) collective-permute-start(bf16[40,2048]{1,0:T(8,128)(2,1)S(1)} %copy-done.14), channel_id=1, source_target_pairs={{0,24},{4,28},{8,0},{12,4},{16,8},{20,12},{24,16},{28,20},{1,25},{... | collective-permute-start | bytes 491528 | tf_op jit(solution)/shard_map/ppermute | solution.py:42
  41.6 12.5 %collective-permute-done.6 = bf16[40,2048]{1,0:T(8,128)(2,1)} collective-permute-done((bf16[40,2048]{1,0:T(8,128)(2,1)}, bf16[40,2048]{1,0:T(8,128)(2,1)}, u32[]{:S(2)}, u32[]{:S(2)}) %collective-permute-start.6) | collective-permute-done | bytes 163872 | tf_op jit(solution)/shard_map/ppermute | solution.py:42
  54.1 7.1 %collective-permute-start.17 = (bf16[40,2048]{1,0:T(8,128)(2,1)S(1)}, bf16[40,2048]{1,0:T(8,128)(2,1)S(1)}, u32[]{:S(2)}, u32[]{:S(2)}) collective-permute-start(bf16[40,2048]{1,0:T(8,128)(2,1)S(1)} %copy-done.13), channel_id=1, source_target_pairs={{0,28},{4,0},{8,4},{12,8},{16,12},{20,16},{24,20},{28,24},{1,29},{... | collective-permute-start | bytes 491528 | tf_op jit(solution)/shard_map/ppermute | solution.py:42
  61.2 1.2 pad_maximum_fusion.2
  63.1 3.0 %collective-permute-done.17 = bf16[40,2048]{1,0:T(8,128)(2,1)S(1)} collective-permute-done((bf16[40,2048]{1,0:T(8,128)(2,1)S(1)}, bf16[40,2048]{1,0:T(8,128)(2,1)S(1)}, u32[]{:S(2)}, u32[]{:S(2)}) %collective-permute-start.17) | collective-permute-done | bytes 163872 | tf_op jit(solution)/shard_map/ppermute | solution.py:42
  66.0 1.0 pad_maximum_fusion.3
  67.0 1.0 collective-permute-start.18
  68.0 1.6 constant_dynamic-update-slice_fusion.3
  69.6 1.6 constant_dynamic-update-slice_fusion.2
  71.2 1.6 constant_dynamic-update-slice_fusion.1
  72.8 10.5 %collective-permute-done.7 = bf16[160,2048]{1,0:T(8,128)(2,1)S(1)} collective-permute-done((bf16[160,2048]{1,0:T(8,128)(2,1)S(1)}, bf16[160,2048]{1,0:T(8,128)(2,1)S(1)}, u32[]{:S(2)}, u32[]{:S(2)}) %collective-permute-start.7) | collective-permute-done | bytes 655392 | tf_op jit(solution)/shard_map/ppermute | solution.py:37
  83.3 1.0 constant_dynamic-update-slice_fusion
  84.3 1.6 constant_dynamic-update-slice_fusion.15
  85.9 0.7 constant_dynamic-update-slice_fusion.14
  86.6 0.7 constant_dynamic-update-slice_fusion.13
  87.3 0.7 constant_dynamic-update-slice_fusion.12
  87.9 2.1 pad_maximum_fusion.1
  90.5 9.5 %collective-permute-done.18 = bf16[160,2048]{1,0:T(8,128)(2,1)S(1)} collective-permute-done((bf16[160,2048]{1,0:T(8,128)(2,1)S(1)}, bf16[160,2048]{1,0:T(8,128)(2,1)S(1)}, u32[]{:S(2)}, u32[]{:S(2)}) %collective-permute-start.18) | collective-permute-done | bytes 655392 | tf_op jit(solution)/shard_map/ppermute | solution.py:37
  100.0 0.9 constant_dynamic-update-slice_fusion.11
  101.1 1.4 copy-done.20
  102.5 1.6 copy-done.19
  104.1 2.6 %fusion.10 = f32[640,512]{1,0:T(8,128)} fusion(bf16[640,2048]{1,0:T(8,128)(2,1)S(1)} %constant_dynamic-update-slice_fusion.5, bf16[1,2048,512]{2,1,0:T(8,128)(2,1)S(1)} %copy-done.33), kind=kOutput, calls=%fused_computation.19 | convolution fusion | flops 1342504960 | bytes 6029312 | tf_op jit(solution)/shard_map/dot_general | solution.py:262
  106.7 7.4 %convolution_convert_fusion.1 = bf16[640,2048]{1,0:T(8,128)(2,1)} fusion(bf16[1,512,2048]{2,1,0:T(8,128)(2,1)S(1)} %copy-done, f32[640,512]{1,0:T(8,128)} %fusion.10, bf16[640,2048]{1,0:T(8,128)(2,1)} %copy-done.19, bf16[1,2048,512]{2,1,0:T(8,128)(2,1)} %param.40), kind=kOutput, calls=%fused_computation.1 | convolution fusion | flops 2688614400 | bytes 10747904 | tf_op jit(solution)/shard_map/dot_general | solution.py:265
  114.1 2.7 %slice.176 = bf16[320,2048]{1,0:T(8,128)(2,1)} slice(bf16[640,2048]{1,0:T(8,128)(2,1)} %convolution_convert_fusion.1), slice={[320:640], [0:2048]} | slice | bytes 2621440 | tf_op jit(solution)/shard_map/slice | solution.py:66
  116.8 1.6 constant_dynamic-update-slice_fusion.16
  118.5 1.6 copy-done.22
  120.1 2.6 %fusion.13 = f32[640,512]{1,0:T(8,128)} fusion(bf16[640,2048]{1,0:T(8,128)(2,1)S(1)} %constant_dynamic-update-slice_fusion.16, bf16[1,2048,512]{2,1,0:T(8,128)(2,1)S(1)} %copy-done.34), kind=kOutput, calls=%fused_computation.20 | convolution fusion | flops 1342504960 | bytes 6029312 | tf_op jit(solution)/shard_map/dot_general | solution.py:262
  122.7 7.3 %convolution_convert_fusion = bf16[640,2048]{1,0:T(8,128)(2,1)} fusion(bf16[1,512,2048]{2,1,0:T(8,128)(2,1)S(1)} %copy-done, f32[640,512]{1,0:T(8,128)} %fusion.13, bf16[640,2048]{1,0:T(8,128)(2,1)} %copy-done.22, bf16[1,2048,512]{2,1,0:T(8,128)(2,1)} %param.40), kind=kOutput, calls=%fused_computation | convolution fusion | flops 2688614400 | bytes 10747904 | tf_op jit(solution)/shard_map/dot_general | solution.py:265
  130.0 1.5 slice.188
  132.0 1.9 convolution_multiply_fusion
  133.9 2.7 %convolution_convert_fusion.4.refs_0_ = bf16[512,256]{1,0:T(8,128)(2,1)} fusion(bf16[1536,256]{1,0:T(8,128)(2,1)S(1)} %copy-done.35, bf16[256,1536]{1,0:T(8,128)(2,1)} %collective-permute-done.1, bf16[128,1536]{1,0:T(8,128)(2,1)} %collective-permute-done, bf16[128,1536]{1,0:T(8,128)(2,1)S(1)} %multiply_convert_fusion.1), kind=kOutput, calls=%fused_computation.39 | convolution fusion | flops 407502848 | bytes 2621440 | tf_op jit(solution)/shard_map/dot_general | solution.py:249
  136.6 1.8 add_convert_fusion.1
  139.5 2.4 fusion.47.refs_1_
  142.5 1.2 collective-permute-start.21
  143.7 12.5 %collective-permute-done.10 = bf16[160,2048]{1,0:T(8,128)(2,1)S(1)} collective-permute-done((bf16[160,2048]{1,0:T(8,128)(2,1)S(1)}, bf16[160,2048]{1,0:T(8,128)(2,1)S(1)}, u32[]{:S(2)}, u32[]{:S(2)}) %collective-permute-start.10) | collective-permute-done | bytes 655392 | tf_op jit(solution)/shard_map/ppermute | solution.py:37
  156.4 9.5 %collective-permute-start.11 = (bf16[40,2048]{1,0:T(8,128)(2,1)S(1)}, bf16[40,2048]{1,0:T(8,128)(2,1)S(1)}, u32[]{:S(2)}, u32[]{:S(2)}) collective-permute-start(bf16[40,2048]{1,0:T(8,128)(2,1)S(1)} %get-tuple-element.20), channel_id=1, source_target_pairs={{0,28},{4,0},{8,4},{12,8},{16,12},{20,16},{24,20},{28,24},{1,29},{... | collective-permute-start | bytes 491528 | tf_op jit(solution)/shard_map/ppermute | solution.py:42
  166.0 3.3 %collective-permute-done.21 = bf16[160,2048]{1,0:T(8,128)(2,1)S(1)} collective-permute-done((bf16[160,2048]{1,0:T(8,128)(2,1)S(1)}, bf16[160,2048]{1,0:T(8,128)(2,1)S(1)}, u32[]{:S(2)}, u32[]{:S(2)}) %collective-permute-start.21) | collective-permute-done | bytes 655392 | tf_op jit(solution)/shard_map/ppermute | solution.py:37
  169.5 0.7 fusion.115
  170.2 5.8 %collective-permute-start.22 = (bf16[40,2048]{1,0:T(8,128)(2,1)S(1)}, bf16[40,2048]{1,0:T(8,128)(2,1)S(1)}, u32[]{:S(2)}, u32[]{:S(2)}) collective-permute-start(bf16[40,2048]{1,0:T(8,128)(2,1)S(1)} %get-tuple-element.15), channel_id=1, source_target_pairs={{0,16},{4,20},{8,24},{12,28},{16,0},{20,4},{24,8},{28,12},{1,17},{... | collective-permute-start | bytes 491528 | tf_op jit(solution)/shard_map/ppermute | solution.py:42
  176.0 4.2 %collective-permute-start.23 = (bf16[40,2048]{1,0:T(8,128)(2,1)S(1)}, bf16[40,2048]{1,0:T(8,128)(2,1)S(1)}, u32[]{:S(2)}, u32[]{:S(2)}) collective-permute-start(bf16[40,2048]{1,0:T(8,128)(2,1)S(1)} %get-tuple-element.14), channel_id=1, source_target_pairs={{0,12},{4,16},{8,20},{12,24},{16,28},{20,0},{24,4},{28,8},{1,13},{... | collective-permute-start | bytes 491528 | tf_op jit(solution)/shard_map/ppermute | solution.py:42
  180.3 0.8 collective-permute-start.25
  181.2 10.5 %collective-permute-done.22 = bf16[40,2048]{1,0:T(8,128)(2,1)S(1)} collective-permute-done((bf16[40,2048]{1,0:T(8,128)(2,1)S(1)}, bf16[40,2048]{1,0:T(8,128)(2,1)S(1)}, u32[]{:S(2)}, u32[]{:S(2)}) %collective-permute-start.22) | collective-permute-done | bytes 163872 | tf_op jit(solution)/shard_map/ppermute | solution.py:42
  191.7 5.1 %collective-permute-done.23 = bf16[40,2048]{1,0:T(8,128)(2,1)S(1)} collective-permute-done((bf16[40,2048]{1,0:T(8,128)(2,1)S(1)}, bf16[40,2048]{1,0:T(8,128)(2,1)S(1)}, u32[]{:S(2)}, u32[]{:S(2)}) %collective-permute-start.23) | collective-permute-done | bytes 163872 | tf_op jit(solution)/shard_map/ppermute | solution.py:42
  196.9 22.7 %attend.1 = bf16[512,256]{1,0:T(8,128)(2,1)} custom-call(bf16[512,256]{1,0:T(8,128)(2,1)} %convolution_convert_fusion.4.refs_0_, bf16[512,128]{1,0:T(8,128)(2,1)} %fusion.47.refs_1_, bf16[4096,640]{1,0:T(8,128)(2,1)} %all-gather.2.cloned.1.call-done.refs_2_, bf16[512,256]{1,0:T(8,128)(2,1)} %refs_3_.1, bf16[512,256]{1,0:T(8,128)(2,1)} %refs_4_.1), custom_call_target="tpu_custom_call" | custom-call | flops 8589934592 | bytes 5242880 | tf_op jit(solution)/shard_map/attend/pallas_call | solution.py:146
  219.6 1.7 convolution_convert_fusion.2
  222.6 1.5 collective-permute-done.2
  225.2 0.9 multiply_convert_fusion
  226.1 12.5 %collective-permute-done.3 = bf16[128,2048]{1,0:T(8,128)(2,1)S(1)} collective-permute-done((bf16[128,2048]{1,0:T(8,128)(2,1)S(1)}, bf16[128,2048]{1,0:T(8,128)(2,1)S(1)}, u32[]{:S(2)}, u32[]{:S(2)}) %collective-permute-start.3) | collective-permute-done | bytes 524320 | tf_op jit(solution)/shard_map/ppermute | solution.py:37
  238.9 1.0 fusion.55
  (153 shorter events, 11.9 us)
Async XLA Ops:
  7.2 99.6 %copy-start = (bf16[1,512,2048]{2,1,0:T(8,128)(2,1)S(1)}, bf16[1,512,2048]{2,1,0:T(8,128)(2,1)}, u32[]{:S(2)}) copy-start(bf16[1,512,2048]{2,1,0:T(8,128)(2,1)} %param.41) | copy-start | bytes 6291460
  7.2 189.7 %all-gather.2.cloned.1.call-start = ((), (), s32[]{:S(2)}) async-start(), calls=%async_computation | async-start | bytes 5406720 | tf_op jit(solution)/shard_map/all_gather | solution.py:242
  8.6 4.1 %copy-start.23 = (f32[1536]{0:T(1024)S(1)}, f32[1536]{0:T(1024)}, u32[]{:S(2)}) copy-start(f32[1536]{0:T(1024)} %param.28) | copy-start | bytes 18436
  8.6 7.3 %copy-start.31 = (s32[4]{0:T(128)S(1)}, s32[4]{0:T(128)}, u32[]{:S(2)}) copy-start(s32[4]{0:T(128)} %constant.75.clone) | copy-start | bytes 52
  12.9 75.0 %collective-permute-start = (bf16[128,1536]{1,0:T(8,128)(2,1)S(1)}, bf16[128,1536]{1,0:T(8,128)(2,1)}, u32[]{:S(2)}, u32[]{:S(2)}) collective-permute-start(bf16[128,1536]{1,0:T(8,128)(2,1)S(1)} %multiply_convert_fusion.1), channel_id=1, source_target_pairs={{0,2},{1,3},{2,0},{3,1},{4,6},{5,7},{6,4},{7,5},{8,10},{9,11},{10,... | collective-permute-start | bytes 1179656 | tf_op jit(solution)/shard_map/ppermute | solution.py:37
  18.4 1.0 copy-start.4
  18.4 1.0 copy-start.24
  19.5 1.6 copy-start.10
  19.5 1.6 copy-start.16
  19.5 2.0 copy-start.32
  22.1 1.3 copy-start.29
  22.1 2.1 copy-start.28
  23.3 2.5 %copy-start.5 = (bf16[128,2048]{1,0:T(8,128)(2,1)S(1)}, bf16[128,2048]{1,0:T(8,128)(2,1)}, u32[]{:S(2)}) copy-start(bf16[128,2048]{1,0:T(8,128)(2,1)} %param.23) | copy-start | bytes 1572868
  23.3 2.7 %copy-start.25 = (f32[2048]{0:T(1024)S(1)}, f32[2048]{0:T(1024)}, u32[]{:S(2)}) copy-start(f32[2048]{0:T(1024)} %param.36) | copy-start | bytes 24580
  26.6 8.1 %copy-start.7 = (bf16[1536,128]{1,0:T(8,128)(2,1)S(1)}, bf16[1536,128]{1,0:T(8,128)(2,1)}, u32[]{:S(2)}) copy-start(bf16[1536,128]{1,0:T(8,128)(2,1)} %param.31) | copy-start | bytes 1179652
  27.8 7.9 %copy-start.30 = (f32[128,2]{0,1:T(2,128)S(1)}, f32[128,2]{0,1:T(2,128)}, u32[]{:S(2)}) copy-start(f32[128,2]{0,1:T(2,128)} %param.38) | copy-start | bytes 3076
  27.8 10.3 %collective-permute-start.4 = (bf16[40,2048]{1,0:T(8,128)(2,1)}, bf16[40,2048]{1,0:T(8,128)(2,1)}, u32[]{:S(2)}, u32[]{:S(2)}) collective-permute-start(bf16[40,2048]{1,0:T(8,128)(2,1)} %get-tuple-element.10), channel_id=1, source_target_pairs={{0,4},{4,8},{8,12},{12,16},{16,20},{20,24},{24,28},{28,0},{1,5},{5... | collective-permute-start | bytes 491528 | tf_op jit(solution)/shard_map/ppermute | solution.py:42
  29.3 9.2 %collective-permute-start.5 = (bf16[40,2048]{1,0:T(8,128)(2,1)}, bf16[40,2048]{1,0:T(8,128)(2,1)}, u32[]{:S(2)}, u32[]{:S(2)}) collective-permute-start(bf16[40,2048]{1,0:T(8,128)(2,1)} %get-tuple-element.9), channel_id=1, source_target_pairs={{0,8},{4,12},{8,16},{12,20},{16,24},{20,28},{24,0},{28,4},{1,9},{5... | collective-permute-start | bytes 491528 | tf_op jit(solution)/shard_map/ppermute | solution.py:42
  30.9 23.2 %collective-permute-start.6 = (bf16[40,2048]{1,0:T(8,128)(2,1)}, bf16[40,2048]{1,0:T(8,128)(2,1)}, u32[]{:S(2)}, u32[]{:S(2)}) collective-permute-start(bf16[40,2048]{1,0:T(8,128)(2,1)} %get-tuple-element.8), channel_id=1, source_target_pairs={{0,12},{4,16},{8,20},{12,24},{16,28},{20,0},{24,4},{28,8},{1,13},{... | collective-permute-start | bytes 491528 | tf_op jit(solution)/shard_map/ppermute | solution.py:42
  33.4 29.0 %collective-permute-start.14 = (bf16[40,2048]{1,0:T(8,128)(2,1)}, bf16[40,2048]{1,0:T(8,128)(2,1)}, u32[]{:S(2)}, u32[]{:S(2)}) collective-permute-start(bf16[40,2048]{1,0:T(8,128)(2,1)} %get-tuple-element.7), channel_id=1, source_target_pairs={{0,16},{4,20},{8,24},{12,28},{16,0},{20,4},{24,8},{28,12},{1,17},{... | collective-permute-start | bytes 491528 | tf_op jit(solution)/shard_map/ppermute | solution.py:42
  34.9 3.2 %copy-start.15 = (bf16[40,2048]{1,0:T(8,128)(2,1)S(1)}, bf16[40,2048]{1,0:T(8,128)(2,1)}, u32[]{:S(2)}) copy-start(bf16[40,2048]{1,0:T(8,128)(2,1)} %get-tuple-element.6) | copy-start | bytes 491524
  34.9 3.6 %copy-start.14 = (bf16[40,2048]{1,0:T(8,128)(2,1)S(1)}, bf16[40,2048]{1,0:T(8,128)(2,1)}, u32[]{:S(2)}) copy-start(bf16[40,2048]{1,0:T(8,128)(2,1)} %get-tuple-element.5) | copy-start | bytes 491524
  34.9 19.2 %copy-start.13 = (bf16[40,2048]{1,0:T(8,128)(2,1)S(1)}, bf16[40,2048]{1,0:T(8,128)(2,1)}, u32[]{:S(2)}) copy-start(bf16[40,2048]{1,0:T(8,128)(2,1)} %get-tuple-element.2) | copy-start | bytes 491524
  38.1 24.9 %collective-permute-start.15 = (bf16[40,2048]{1,0:T(8,128)(2,1)S(1)}, bf16[40,2048]{1,0:T(8,128)(2,1)S(1)}, u32[]{:S(2)}, u32[]{:S(2)}) collective-permute-start(bf16[40,2048]{1,0:T(8,128)(2,1)S(1)} %copy-done.15), channel_id=1, source_target_pairs={{0,20},{4,24},{8,28},{12,0},{16,4},{20,8},{24,12},{28,16},{1,21},{... | collective-permute-start | bytes 491528 | tf_op jit(solution)/shard_map/ppermute | solution.py:42
  38.5 24.5 %collective-permute-start.16 = (bf16[40,2048]{1,0:T(8,128)(2,1)S(1)}, bf16[40,2048]{1,0:T(8,128)(2,1)S(1)}, u32[]{:S(2)}, u32[]{:S(2)}) collective-permute-start(bf16[40,2048]{1,0:T(8,128)(2,1)S(1)} %copy-done.14), channel_id=1, source_target_pairs={{0,24},{4,28},{8,0},{12,4},{16,8},{20,12},{24,16},{28,20},{1,25},{... | collective-permute-start | bytes 491528 | tf_op jit(solution)/shard_map/ppermute | solution.py:42
  54.1 11.9 %collective-permute-start.17 = (bf16[40,2048]{1,0:T(8,128)(2,1)S(1)}, bf16[40,2048]{1,0:T(8,128)(2,1)S(1)}, u32[]{:S(2)}, u32[]{:S(2)}) collective-permute-start(bf16[40,2048]{1,0:T(8,128)(2,1)S(1)} %copy-done.13), channel_id=1, source_target_pairs={{0,28},{4,0},{8,4},{12,8},{16,12},{20,16},{24,20},{28,24},{1,29},{... | collective-permute-start | bytes 491528 | tf_op jit(solution)/shard_map/ppermute | solution.py:42
  61.2 6.8 %copy-start.17 = (bf16[320,2048]{1,0:T(8,128)(2,1)S(1)}, bf16[320,2048]{1,0:T(8,128)(2,1)}, u32[]{:S(2)}) copy-start(bf16[320,2048]{1,0:T(8,128)(2,1)} %get-tuple-element.3) | copy-start | bytes 3932164
  62.5 20.8 %collective-permute-start.7 = (bf16[160,2048]{1,0:T(8,128)(2,1)S(1)}, bf16[160,2048]{1,0:T(8,128)(2,1)S(1)}, u32[]{:S(2)}, u32[]{:S(2)}) collective-permute-start(bf16[160,2048]{1,0:T(8,128)(2,1)S(1)} %pad_maximum_fusion.2), channel_id=1, source_target_pairs={{0,2},{1,3},{2,0},{3,1},{4,6},{5,7},{6,4},{7,5},{8,10},{9,11},{10,... | collective-permute-start | bytes 1966088 | tf_op jit(solution)/shard_map/ppermute | solution.py:37
  67.0 33.0 %collective-permute-start.18 = (bf16[160,2048]{1,0:T(8,128)(2,1)S(1)}, bf16[160,2048]{1,0:T(8,128)(2,1)S(1)}, u32[]{:S(2)}, u32[]{:S(2)}) collective-permute-start(bf16[160,2048]{1,0:T(8,128)(2,1)S(1)} %pad_maximum_fusion.3), channel_id=1, source_target_pairs={{0,2},{1,3},{2,0},{3,1},{4,6},{5,7},{6,4},{7,5},{8,10},{9,11},{10,... | collective-permute-start | bytes 1966088 | tf_op jit(solution)/shard_map/ppermute | solution.py:37
  84.3 16.7 %collective-permute-start.8 = (bf16[320,2048]{1,0:T(8,128)(2,1)S(1)}, bf16[320,2048]{1,0:T(8,128)(2,1)S(1)}, u32[]{:S(2)}, u32[]{:S(2)}) collective-permute-start(bf16[320,2048]{1,0:T(8,128)(2,1)S(1)} %get-tuple-element.22), channel_id=1, source_target_pairs={{0,1},{1,0},{2,3},{3,2},{4,5},{5,4},{6,7},{7,6},{8,9},{9,8},{10,11... | collective-permute-start | bytes 3932168 | tf_op jit(solution)/shard_map/ppermute | solution.py:37
  87.9 13.0 %copy-start.18 = (bf16[640,2048]{1,0:T(8,128)(2,1)S(1)}, bf16[640,2048]{1,0:T(8,128)(2,1)}, u32[]{:S(2)}) copy-start(bf16[640,2048]{1,0:T(8,128)(2,1)} %get-tuple-element.23) | copy-start | bytes 7864324
  90.0 42.0 %collective-permute-start.1 = (bf16[256,1536]{1,0:T(8,128)(2,1)}, bf16[256,1536]{1,0:T(8,128)(2,1)}, u32[]{:S(2)}, u32[]{:S(2)}) collective-permute-start(bf16[256,1536]{1,0:T(8,128)(2,1)} %pad_maximum_fusion.1), channel_id=1, source_target_pairs={{0,1},{1,0},{2,3},{3,2},{4,5},{5,4},{6,7},{7,6},{8,9},{9,8},{10,11... | collective-permute-start | bytes 2359304 | tf_op jit(solution)/shard_map/ppermute | solution.py:37
  101.0 1.6 copy-start.20
  101.0 15.9 %collective-permute-start.19 = (bf16[320,2048]{1,0:T(8,128)(2,1)}, bf16[320,2048]{1,0:T(8,128)(2,1)}, u32[]{:S(2)}, u32[]{:S(2)}) collective-permute-start(bf16[320,2048]{1,0:T(8,128)(2,1)} %get-tuple-element.16), channel_id=1, source_target_pairs={{0,1},{1,0},{2,3},{3,2},{4,5},{5,4},{6,7},{7,6},{8,9},{9,8},{10,11... | collective-permute-start | bytes 3932168 | tf_op jit(solution)/shard_map/ppermute | solution.py:37
  101.0 3.2 %copy-start.33 = (bf16[1,2048,512]{2,1,0:T(8,128)(2,1)S(1)}, bf16[1,2048,512]{2,1,0:T(8,128)(2,1)}, u32[]{:S(2)}) copy-start(bf16[1,2048,512]{2,1,0:T(8,128)(2,1)} %param.39) | copy-start | bytes 6291460
  102.5 1.6 copy-start.19
  114.1 2.8 %copy-start.21 = (bf16[640,2048]{1,0:T(8,128)(2,1)S(1)}, bf16[640,2048]{1,0:T(8,128)(2,1)}, u32[]{:S(2)}) copy-start(bf16[640,2048]{1,0:T(8,128)(2,1)} %copy-done.20) | copy-start | bytes 7864324
  116.8 19.8 %collective-permute-start.9 = (bf16[320,2048]{1,0:T(8,128)(2,1)}, bf16[320,2048]{1,0:T(8,128)(2,1)}, u32[]{:S(2)}, u32[]{:S(2)}) collective-permute-start(bf16[320,2048]{1,0:T(8,128)(2,1)} %slice.176), channel_id=1, source_target_pairs={{0,1},{1,0},{2,3},{3,2},{4,5},{5,4},{6,7},{7,6},{8,9},{9,8},{10,11... | collective-permute-start | bytes 3932168 | tf_op jit(solution)/shard_map/ppermute | solution.py:37
  116.8 3.2 %copy-start.34 = (bf16[1,2048,512]{2,1,0:T(8,128)(2,1)S(1)}, bf16[1,2048,512]{2,1,0:T(8,128)(2,1)}, u32[]{:S(2)}) copy-start(bf16[1,2048,512]{2,1,0:T(8,128)(2,1)} %param.39) | copy-start | bytes 6291460
  118.5 1.6 copy-start.22
  130.0 2.0 copy-start.9
  130.0 2.0 copy-start.12
  131.5 10.4 %collective-permute-start.20 = (bf16[320,2048]{1,0:T(8,128)(2,1)S(1)}, bf16[320,2048]{1,0:T(8,128)(2,1)S(1)}, u32[]{:S(2)}, u32[]{:S(2)}) collective-permute-start(bf16[320,2048]{1,0:T(8,128)(2,1)S(1)} %slice.188), channel_id=1, source_target_pairs={{0,1},{1,0},{2,3},{3,2},{4,5},{5,4},{6,7},{7,6},{8,9},{9,8},{10,11... | collective-permute-start | bytes 3932168 | tf_op jit(solution)/shard_map/ppermute | solution.py:37
  132.0 1.9 copy-start.35
  133.9 2.7 %copy-start.3 = (bf16[640,2048]{1,0:T(8,128)(2,1)S(1)}, bf16[640,2048]{1,0:T(8,128)(2,1)}, u32[]{:S(2)}) copy-start(bf16[640,2048]{1,0:T(8,128)(2,1)} %convolution_convert_fusion.1) | copy-start | bytes 7864324
  138.4 1.0 copy-start.8
  138.4 1.1 copy-start.11
  138.5 3.4 %copy-start.2 = (bf16[640,2048]{1,0:T(8,128)(2,1)S(1)}, bf16[640,2048]{1,0:T(8,128)(2,1)}, u32[]{:S(2)}) copy-start(bf16[640,2048]{1,0:T(8,128)(2,1)} %convolution_convert_fusion) | copy-start | bytes 7864324
  138.5 17.7 %collective-permute-start.10 = (bf16[160,2048]{1,0:T(8,128)(2,1)S(1)}, bf16[160,2048]{1,0:T(8,128)(2,1)S(1)}, u32[]{:S(2)}, u32[]{:S(2)}) collective-permute-start(bf16[160,2048]{1,0:T(8,128)(2,1)S(1)} %slice.178), channel_id=1, source_target_pairs={{0,2},{1,3},{2,0},{3,1},{4,6},{5,7},{6,4},{7,5},{8,10},{9,11},{10,... | collective-permute-start | bytes 1966088 | tf_op jit(solution)/shard_map/ppermute | solution.py:37
  142.5 26.8 %collective-permute-start.21 = (bf16[160,2048]{1,0:T(8,128)(2,1)S(1)}, bf16[160,2048]{1,0:T(8,128)(2,1)S(1)}, u32[]{:S(2)}, u32[]{:S(2)}) collective-permute-start(bf16[160,2048]{1,0:T(8,128)(2,1)S(1)} %slice.190), channel_id=1, source_target_pairs={{0,2},{1,3},{2,0},{3,1},{4,6},{5,7},{6,4},{7,5},{8,10},{9,11},{10,... | collective-permute-start | bytes 1966088 | tf_op jit(solution)/shard_map/ppermute | solution.py:37
  156.4 23.8 %collective-permute-start.11 = (bf16[40,2048]{1,0:T(8,128)(2,1)S(1)}, bf16[40,2048]{1,0:T(8,128)(2,1)S(1)}, u32[]{:S(2)}, u32[]{:S(2)}) collective-permute-start(bf16[40,2048]{1,0:T(8,128)(2,1)S(1)} %get-tuple-element.20), channel_id=1, source_target_pairs={{0,28},{4,0},{8,4},{12,8},{16,12},{20,16},{24,20},{28,24},{1,29},{... | collective-permute-start | bytes 491528 | tf_op jit(solution)/shard_map/ppermute | solution.py:42
  166.0 14.3 %collective-permute-start.12 = (bf16[40,2048]{1,0:T(8,128)(2,1)S(1)}, bf16[40,2048]{1,0:T(8,128)(2,1)S(1)}, u32[]{:S(2)}, u32[]{:S(2)}) collective-permute-start(bf16[40,2048]{1,0:T(8,128)(2,1)S(1)} %get-tuple-element.19), channel_id=1, source_target_pairs={{0,24},{4,28},{8,0},{12,4},{16,8},{20,12},{24,16},{28,20},{1,25},{... | collective-permute-start | bytes 491528 | tf_op jit(solution)/shard_map/ppermute | solution.py:42
  166.0 15.2 %collective-permute-start.13 = (bf16[40,2048]{1,0:T(8,128)(2,1)S(1)}, bf16[40,2048]{1,0:T(8,128)(2,1)S(1)}, u32[]{:S(2)}, u32[]{:S(2)}) collective-permute-start(bf16[40,2048]{1,0:T(8,128)(2,1)S(1)} %get-tuple-element.18), channel_id=1, source_target_pairs={{0,20},{4,24},{8,28},{12,0},{16,4},{20,8},{24,12},{28,16},{1,21},{... | collective-permute-start | bytes 491528 | tf_op jit(solution)/shard_map/ppermute | solution.py:42
  170.2 21.5 %collective-permute-start.22 = (bf16[40,2048]{1,0:T(8,128)(2,1)S(1)}, bf16[40,2048]{1,0:T(8,128)(2,1)S(1)}, u32[]{:S(2)}, u32[]{:S(2)}) collective-permute-start(bf16[40,2048]{1,0:T(8,128)(2,1)S(1)} %get-tuple-element.15), channel_id=1, source_target_pairs={{0,16},{4,20},{8,24},{12,28},{16,0},{20,4},{24,8},{28,12},{1,17},{... | collective-permute-start | bytes 491528 | tf_op jit(solution)/shard_map/ppermute | solution.py:42
  176.0 20.8 %collective-permute-start.23 = (bf16[40,2048]{1,0:T(8,128)(2,1)S(1)}, bf16[40,2048]{1,0:T(8,128)(2,1)S(1)}, u32[]{:S(2)}, u32[]{:S(2)}) collective-permute-start(bf16[40,2048]{1,0:T(8,128)(2,1)S(1)} %get-tuple-element.14), channel_id=1, source_target_pairs={{0,12},{4,16},{8,20},{12,24},{16,28},{20,0},{24,4},{28,8},{1,13},{... | collective-permute-start | bytes 491528 | tf_op jit(solution)/shard_map/ppermute | solution.py:42
  180.2 41.2 %collective-permute-start.24 = (bf16[40,2048]{1,0:T(8,128)(2,1)}, bf16[40,2048]{1,0:T(8,128)(2,1)S(1)}, u32[]{:S(2)}, u32[]{:S(2)}) collective-permute-start(bf16[40,2048]{1,0:T(8,128)(2,1)} %get-tuple-element.13), channel_id=1, source_target_pairs={{0,8},{4,12},{8,16},{12,20},{16,24},{20,28},{24,0},{28,4},{1,9},{5... | collective-permute-start | bytes 491528 | tf_op jit(solution)/shard_map/ppermute | solution.py:42
  180.3 41.2 %collective-permute-start.25 = (bf16[40,2048]{1,0:T(8,128)(2,1)S(1)}, bf16[40,2048]{1,0:T(8,128)(2,1)S(1)}, u32[]{:S(2)}, u32[]{:S(2)}) collective-permute-start(bf16[40,2048]{1,0:T(8,128)(2,1)S(1)} %get-tuple-element.12), channel_id=1, source_target_pairs={{0,4},{4,8},{8,12},{12,16},{16,20},{20,24},{24,28},{28,0},{1,5},{5... | collective-permute-start | bytes 491528 | tf_op jit(solution)/shard_map/ppermute | solution.py:42
  196.9 22.7 %copy-start.6 = (bf16[256,2048]{1,0:T(8,128)(2,1)S(1)}, bf16[256,2048]{1,0:T(8,128)(2,1)}, u32[]{:S(2)}) copy-start(bf16[256,2048]{1,0:T(8,128)(2,1)} %param.34) | copy-start | bytes 3145732
  221.4 2.7 %collective-permute-start.2 = (bf16[256,2048]{1,0:T(8,128)(2,1)S(1)}, bf16[256,2048]{1,0:T(8,128)(2,1)S(1)}, u32[]{:S(2)}, u32[]{:S(2)}) collective-permute-start(bf16[256,2048]{1,0:T(8,128)(2,1)S(1)} %slice.167), channel_id=1, source_target_pairs={{0,1},{1,0},{2,3},{3,2},{4,5},{5,4},{6,7},{7,6},{8,9},{9,8},{10,11... | collective-permute-start | bytes 3145736 | tf_op jit(solution)/shard_map/ppermute | solution.py:37
  222.6 2.6 %copy-start.26 = (f32[2048]{0:T(1024)S(1)}, f32[2048]{0:T(1024)}, u32[]{:S(2)}) copy-start(f32[2048]{0:T(1024)} %param.42) | copy-start | bytes 24580
  224.6 14.0 %collective-permute-start.3 = (bf16[128,2048]{1,0:T(8,128)(2,1)S(1)}, bf16[128,2048]{1,0:T(8,128)(2,1)S(1)}, u32[]{:S(2)}, u32[]{:S(2)}) collective-permute-start(bf16[128,2048]{1,0:T(8,128)(2,1)S(1)} %slice.169), channel_id=1, source_target_pairs={{0,2},{1,3},{2,0},{3,1},{4,6},{5,7},{6,4},{7,5},{8,10},{9,11},{10,... | collective-permute-start | bytes 1572872 | tf_op jit(solution)/shard_map/ppermute | solution.py:37
  225.2 13.7 %copy-start.27 = (f32[2048]{0:T(1024)S(1)}, f32[2048]{0:T(1024)}, u32[]{:S(2)}) copy-start(f32[2048]{0:T(1024)} %param.35) | copy-start | bytes 24580
  225.2 14.7 %copy-start.1 = (bf16[1,512,2048]{2,1,0:T(8,128)(2,1)S(1)}, bf16[1,512,2048]{2,1,0:T(8,128)(2,1)}, u32[]{:S(2)}) copy-start(bf16[1,512,2048]{2,1,0:T(8,128)(2,1)} %param.41) | copy-start | bytes 6291460
Sparse Core Ops, SparseCore 0:
  24.3 86.8 all-gather.1
